TPU v7x, 1024 devices: a whole 4x4x32 slice. The times are simulated.
1024 devices in a mesh: kv: 256 (over z, x, core), tp: 4 (over y).
Axes of the slice: x: 4, y: 4, z: 32, core: 2. Of those that a mesh axis runs over, the one named last changes fastest.
Arguments:
- hidden_in: bfloat16 [4, 16384, 2048], P(None, 'kv'), may hold values from -84 to 84
- w_query: bfloat16 [2048, 1024], P(None, 'tp'), may hold values from -0.125 to 0.125
- w_cmp_key: bfloat16 [2048, 256], P(None, 'tp'), may hold values from -0.125 to 0.125
- w_cmp_value: bfloat16 [2048, 256], P(None, 'tp'), may hold values from -0.8838835 to 0.8838835
- w_sel_key: bfloat16 [2048, 256], P(None, 'tp'), may hold values from -0.125 to 0.125
- w_sel_value: bfloat16 [2048, 256], P(None, 'tp'), may hold values from -0.8838835 to 0.8838835
- w_gate: bfloat16 [2048, 2, 16], replicated, may hold values from -0.125 to 0.125
- cmp_key_in: bfloat16 [2048, 128], replicated, may hold values from -0.125 to 0.125
- cmp_key_out: bfloat16 [128, 64], replicated, may hold values from -0.5 to 0.5
- cmp_value_in: bfloat16 [2048, 128], replicated, may hold values from -0.125 to 0.125
- cmp_value_out: bfloat16 [128, 64], replicated, may hold values from -0.5 to 0.5
- out_gain: float32 [1024], replicated, may hold values from 0.1 to 1.9
- w_out: bfloat16 [1024, 2048], replicated, may hold values from -0.1875 to 0.1875
- seq_lengths: int32 [4], replicated, may hold values from 1 to 16384, 26214 in all
- chosen: int32 [4, 256, 4, 16], P(None, 'kv', 'tp'), may hold values from -1 to 255, as said below
Outputs:
- attended: bfloat16 [4, 16384, 2048], P(None, 'kv', 'tp')
Inputs may be any that keep to these rules, and one draw needn't show every extreme that they name: chosen[s, b, g, 0] is b itself. Every other entry is -1 or a block index below b, and the entries of one list that are not -1 are distinct. For each block index and key group, the entries after the first slot that name that index all lie in the lists of a single sequence.
All inputs are finite; a program needn't handle non-finite values.
Results may differ from a plain program's by a relative error of at most 0.012.
The roundings to bfloat16 on the way count: a program that leaves them out, or rounds other values in their place, can miss the bound.
Values may be sent and summed in bfloat16 or wider, within the bound.
A program may use at most 64 MiB of HBM per device.

v0:
```python
import functools

import jax
import jax.numpy as jnp
from jax import lax
from jax.sharding import Mesh
from jax.sharding import PartitionSpec as P

HEADS = 16
HEAD_DIM = 64
CMP_STRIDE = 16
CMP_BLOCK = 32
TOPK = 16
KV = ("kv_0", "kv_1", "kv_2")


theta_base = 500000.0
norm_eps = 1e-06


def by_axis(array, axes):
    return functools.reduce(lax.pmax, axes, array)


def turned_gather(arrays, axis, dims):
    turned = [jnp.moveaxis(a, dim, 0) for a, dim in zip(arrays, dims)]
    widths = [t[0].size for t in turned]
    both = jnp.concatenate([t.reshape(-1, w) for t, w in zip(turned, widths)], axis=1)
    filled = lax.all_gather(both, axis, axis=0, tiled=True)
    tiles = jnp.split(filled, [sum(widths[:k]) for k in range(1, len(widths))], axis=1)
    return tuple(
        (
            jnp.moveaxis(b.reshape(-1, *t.shape[1:]), 0, dim)
            for b, t, dim in zip(tiles, turned, dims)
        )
    )


def rotate(values, positions):
    width = values.shape[-1]
    half = width // 2
    inverse = jnp.exp(
        -jnp.log(jnp.float32(theta_base)) * jnp.arange(0, width, 2).astype(jnp.float32) / width
    )
    angle = positions.astype(jnp.float32)[:, None] * inverse[None, :]
    cosine = jnp.cos(angle)[:, None, :]
    sine = jnp.sin(angle)[:, None, :]
    first = values[..., :half]
    second = values[..., half:]
    return jnp.concatenate(
        [first * cosine - second * sine, second * cosine + first * sine], axis=-1
    )


def masked_weights(scores, valid):
    top = jnp.max(jnp.where(valid, scores, -1e30), axis=-1, keepdims=True)
    expd = jnp.where(valid, jnp.exp(scores - top), 0.0)
    total = jnp.sum(expd, axis=-1, keepdims=True)
    return (expd / jnp.maximum(total, 1.0)).astype(jnp.bfloat16)


def compress(raw, prior, weight_in, weight_out):
    seqs, span, groups, width = raw.shape
    extended = jnp.concatenate([prior, raw], axis=1)
    count = span // CMP_STRIDE
    front = extended[:, :span].reshape(seqs, count, CMP_STRIDE, groups, width)
    back = extended[:, CMP_STRIDE:].reshape(seqs, count, CMP_STRIDE, groups, width)
    window = jnp.concatenate([front, back], axis=2).transpose(0, 1, 3, 2, 4)
    window = window.reshape(seqs * count * groups, CMP_BLOCK * width)
    inner = jax.nn.gelu(jnp.dot(window, weight_in, preferred_element_type=jnp.float32)).astype(
        jnp.bfloat16
    )
    return jnp.dot(inner, weight_out, preferred_element_type=jnp.float32).reshape(
        seqs, count, groups, width
    )


def shards(
    hidden_in,
    w_query,
    w_cmp_key,
    w_cmp_value,
    w_sel_key,
    w_sel_value,
    w_gate,
    cmp_key_in,
    cmp_key_out,
    cmp_value_in,
    cmp_value_out,
    out_gain,
    w_out,
    seq_lengths,
    chosen,
):
    seqs, span, width = hidden_in.shape
    block_list = lax.axis_size(KV)
    place = lax.axis_index(KV)
    column = lax.axis_index("tp")
    local_heads = w_query.shape[1] // HEAD_DIM
    local_groups = w_sel_key.shape[1] // HEAD_DIM
    per_group = local_heads // local_groups
    count = span // CMP_STRIDE
    scale = HEAD_DIM ** (-0.5)
    rows = hidden_in.reshape(seqs * span, width)
    positions = place * span + jnp.arange(span, dtype=jnp.int32)

    def project(weight_matrix, heads):
        return jnp.dot(rows, weight_matrix, preferred_element_type=jnp.float32).reshape(
            seqs, span, heads, HEAD_DIM
        )

    queries = rotate(project(w_query, local_heads), positions).astype(jnp.bfloat16)
    sel_pairs = jnp.concatenate(
        [rotate(project(w_sel_key, local_groups), positions), project(w_sel_value, local_groups)],
        axis=-1,
    ).astype(jnp.bfloat16)
    raw_pairs = jnp.concatenate(
        [project(w_cmp_key, local_groups), project(w_cmp_value, local_groups)], axis=-1
    ).astype(jnp.bfloat16)
    prior = jnp.zeros((seqs, CMP_STRIDE, local_groups, HEAD_DIM), jnp.bfloat16)
    ends = place * span + jnp.arange(count, dtype=jnp.int32) * CMP_STRIDE + CMP_STRIDE - 1
    cmp_keys = rotate(compress(raw_pairs[..., :HEAD_DIM], prior, cmp_key_in, cmp_key_out), ends)
    cmp_values = compress(raw_pairs[..., HEAD_DIM:], prior, cmp_value_in, cmp_value_out)
    cmp_piece = jnp.concatenate(
        [cmp_keys.astype(jnp.bfloat16), cmp_values.astype(jnp.bfloat16)], axis=-1
    )[:, None]
    picks = chosen[:, 0]
    wanted = jnp.any(
        picks[:, :, 1:, None] == jnp.arange(block_list, dtype=jnp.int32), axis=2
    ).astype(jnp.int32)
    wanted = by_axis(wanted, KV)
    named = lax.dynamic_index_in_dim(wanted, place, axis=2, keepdims=False)
    seq_ids = jnp.arange(seqs, dtype=jnp.int32)[:, None]
    exported_seq = jnp.sum(named * seq_ids, axis=0)
    selector = seq_ids == exported_seq[None, :]
    export = jnp.sum(
        jnp.where(selector[:, None, :, None], sel_pairs, jnp.zeros((), jnp.bfloat16)), axis=0
    )
    export = export[None]
    remote_pairs, remote_entries = turned_gather((export, cmp_piece), KV, (0, 1))
    gate_all = jnp.dot(rows, w_gate.reshape(width, 2 * HEADS), preferred_element_type=jnp.float32)
    gate_all = gate_all.reshape(seqs, span, 2, HEADS)
    gates = jax.nn.sigmoid(lax.dynamic_slice_in_dim(gate_all, column * local_heads, local_heads, 3))
    entry = jnp.arange(block_list * count, dtype=jnp.int32)
    entry_end = entry * CMP_STRIDE + CMP_STRIDE - 1
    cmp_valid = ((entry >= 1)[None, :] & (entry_end[None, :] <= positions[:, None]))[None, None]
    key_pos = jnp.arange(span, dtype=jnp.int32)
    own_valid = key_pos[None, :] <= key_pos[:, None]

    def one_sequence(args):
        seq_queries, seq_entries, seq_picks, seq_pairs, seq_gates, seq_length = args
        block_q = seq_queries.reshape(span, local_groups, per_group, HEAD_DIM)
        entries = seq_entries.reshape(block_list * count, local_groups, 2 * HEAD_DIM)
        scores = (
            jnp.einsum(
                "qghd,egd->ghqe",
                block_q,
                entries[..., :HEAD_DIM],
                preferred_element_type=jnp.float32,
            )
            * scale
        )
        weights = masked_weights(scores, cmp_valid)
        cmp_out = jnp.einsum(
            "ghqe,egd->qghd", weights, entries[..., HEAD_DIM:], preferred_element_type=jnp.float32
        )
        far = jnp.maximum(seq_picks[:, 1:], 0)
        fetched = jax.vmap(lambda table, index: table[index], in_axes=(2, 0))(remote_pairs, far)
        near = jnp.transpose(seq_pairs, (1, 0, 2))[:, None]
        pairs = jnp.concatenate([near, fetched], axis=1).reshape(
            local_groups, TOPK * span, 2 * HEAD_DIM
        )
        far_live = jnp.broadcast_to(
            (seq_picks[:, 1:] >= 0)[:, None, :, None], (local_groups, span, TOPK - 1, span)
        )
        near_live = own_valid[None, :, None, :]
        sel_valid = jnp.concatenate([near_live, far_live], axis=2).reshape(
            local_groups, 1, span, TOPK * span
        )
        scores_s = (
            jnp.einsum(
                "qghd,gmd->ghqm", block_q, pairs[..., :HEAD_DIM], preferred_element_type=jnp.float32
            )
            * scale
        )
        weights_s = masked_weights(scores_s, sel_valid)
        sel_out = jnp.einsum(
            "ghqm,gmd->qghd", weights_s, pairs[..., HEAD_DIM:], preferred_element_type=jnp.float32
        )
        split = seq_gates.reshape(span, 2, local_groups, per_group, 1)
        mixed = split[:, 0] * cmp_out + split[:, 1] * sel_out
        mixed = jnp.where((positions < seq_length)[:, None, None, None], mixed, 0.0)
        return mixed.reshape(span, local_heads * HEAD_DIM).astype(jnp.bfloat16)

    mixed = lax.map(one_sequence, (queries, remote_entries, picks, sel_pairs, gates, seq_lengths))
    mixed = mixed.reshape(seqs * span, local_heads * HEAD_DIM)
    out_width = width // lax.axis_size("tp")
    own_columns = lax.dynamic_slice_in_dim(w_out, column * out_width, out_width, 1)
    piece_wide = lax.all_gather(mixed, "tp", axis=1, tiled=True).astype(jnp.float32)
    scaled_piece = (piece_wide * out_gain[None, :]).astype(jnp.bfloat16)
    total = jnp.dot(scaled_piece, own_columns, preferred_element_type=jnp.float32)
    squares = jnp.sum(piece_wide * piece_wide, axis=-1)
    row_scale = lax.rsqrt(squares / (HEADS * HEAD_DIM) + norm_eps)
    return (total * row_scale[:, None]).astype(jnp.bfloat16).reshape(seqs, span, out_width)


def solution(mesh):
    torus = Mesh(mesh.devices.reshape(32, 4, 2, mesh.shape["tp"]), ("kv_0", "kv_1", "kv_2", "tp"))
    return jax.shard_map(
        shards,
        mesh=torus,
        in_specs=(
            P(None, KV, None),
            P(None, "tp"),
            P(None, "tp"),
            P(None, "tp"),
            P(None, "tp"),
            P(None, "tp"),
            P(),
            P(),
            P(),
            P(),
            P(),
            P(),
            P(),
            P(),
            P(None, KV, "tp", None),
        ),
        out_specs=P(None, KV, "tp"),
        check_vma=False,
    )
```

profile of v0, /device:TPU:1, one launch (start us, length us, event | category | flops | bytes accessed | tf_op | source)
XLA Modules:
  0.0 437.6 jit_solution(8793269933719835344)
XLA Ops:
  6.7 1.0 copy-done
  7.8 1.6 convolution_bitcast_fusion.2
  9.7 0.8 slice_bitcast_fusion.10
  10.7 42.0 %pmax.21 = s32[4,1,256]{2,0,1:T(4,128)S(1)} all-reduce(s32[4,1,256]{2,0,1:T(4,128)S(1)} %convert_bitcast_fusion), channel_id=1, replica_groups=mesh['kv_0'=32,'kv_1'=4,'kv_2'=2,'tp'=4] {'kv_0'}, use_global_device_ids=true, to_apply=%region_1.0 | all-reduce | flops 1024 | bytes 8192 | tf_op jit(solution)/shard_map/pmax | solution.py:22
  52.7 7.2 %pmax.22 = s32[4,1,256]{2,0,1:T(4,128)S(1)} all-reduce(s32[4,1,256]{2,0,1:T(4,128)S(1)} %pmax.21), channel_id=1, replica_groups=mesh['kv_0'=32,'kv_1'=4,'kv_2'=2,'tp'=4] {'kv_1'}, use_global_device_ids=true, to_apply=%region_2.0 | all-reduce | flops 1024 | bytes 8192 | tf_op jit(solution)/shard_map/pmax | solution.py:22
  59.8 8.5 %pmax.23 = s32[4,1,256]{2,0,1:T(4,128)S(1)} all-reduce(s32[4,1,256]{2,0,1:T(4,128)S(1)} %pmax.22), channel_id=1, replica_groups=mesh['kv_0'=32,'kv_1'=4,'kv_2'=2,'tp'=4] {'kv_2'}, use_global_device_ids=true, to_apply=%region_3.0 | all-reduce | flops 1024 | bytes 8192 | tf_op jit(solution)/shard_map/pmax | solution.py:22
  68.5 0.6 fusion.74
  69.1 0.6 iota_compare_fusion.3
  69.8 1.4 fusion.30
  71.3 0.6 copy.129
  71.9 0.7 multiply_cosine_fusion.1
  72.6 1.6 convolution_convert_fusion.1
  74.7 1.6 convolution_convert_fusion
  76.9 1.0 fusion.63
  77.9 0.8 subtract_convert_fusion.2
  78.7 1.0 convolution_convert_fusion.3
  79.8 1.4 maximum_bitcast_fusion.1
  81.3 0.6 copy.105
  82.0 1.5 fusion.35
  83.5 0.7 fusion.33
  84.4 263.3 %all-gather.3.cloned.1.call-done = bf16[256,1,10240]{2,1,0:T(2,128)(2,1)} async-done(((bf16[1,1,10240]{2,1,0:T(2,128)(2,1)}), bf16[256,1,10240]{2,1,0:T(2,128)(2,1)}) %all-gather.3.cloned.1.call-update) | async-done | bytes 5242896 | tf_op jit(solution)/shard_map/all_gather | solution.py:29
  347.7 6.9 %copy.127 = bf16[256,1,10240]{2,0,1:T(8,128)(2,1)S(1)} copy(bf16[256,1,10240]{2,1,0:T(2,128)(2,1)} %all-gather.3.cloned.1.call-done) | data formatting | bytes 10485760
  354.6 2.2 split.9
  356.9 0.8 reshape.570
  358.1 58.8 %while.11 = (s32[]{:T(128)}, bf16[4,64,256]{2,1,0:T(8,128)(2,1)}, s32[4]{0:T(128)S(1)}, f32[4,64,2,4]{1,3,2,0:T(4,128)S(1)}, bf16[4,256,4,1,128]{4,2,1,3,0:T(4,1...) while((s32[]{:T(128)}, bf16[4,64,256]{2,1,0:T(8,128)(2,1)}, ...), condition=%wide.region_11.12_spmd.clone, body=%wide.region_6.11_spmd.clone.sunk | while | flops 139874016 | bytes 18430860 | solution.py:195
  358.1 0.7 fusion.111
  358.8 5.4 %copy.134 = bf16[32,8,64,128]{3,2,1,0:T(8,128)(2,1)} copy(bf16[32,8,64,128]{3,1,2,0:T(8,128)(2,1)} %bitcast.247) | data formatting | bytes 8388608 | tf_op jit(solution)/shard_map/while
  364.2 2.8 gather_fusion
  367.6 0.4 select_reduce_fusion.5
  368.4 0.7 fusion.113
  369.3 0.4 select_reduce_fusion.6
  370.1 0.6 dynamic_slice.78
  370.7 0.6 add_compare_fusion.2
  371.4 0.7 fusion.115
  372.2 0.6 constant_dynamic-update-slice_fusion.2
  372.8 0.7 fusion.111
  373.5 5.4 %copy.134 = bf16[32,8,64,128]{3,2,1,0:T(8,128)(2,1)} copy(bf16[32,8,64,128]{3,1,2,0:T(8,128)(2,1)} %bitcast.247) | data formatting | bytes 8388608 | tf_op jit(solution)/shard_map/while
  378.9 2.8 gather_fusion
  383.1 0.7 fusion.113
  384.0 0.4 select_reduce_fusion.6
  384.8 0.6 dynamic_slice.78
  385.4 0.6 add_compare_fusion.2
  386.1 0.7 fusion.115
  386.8 0.6 constant_dynamic-update-slice_fusion.2
  387.5 0.7 fusion.111
  388.2 5.4 %copy.134 = bf16[32,8,64,128]{3,2,1,0:T(8,128)(2,1)} copy(bf16[32,8,64,128]{3,1,2,0:T(8,128)(2,1)} %bitcast.247) | data formatting | bytes 8388608 | tf_op jit(solution)/shard_map/while
  393.6 2.8 gather_fusion
  397.8 0.7 fusion.113
  398.7 0.4 select_reduce_fusion.6
  399.5 0.6 dynamic_slice.78
  400.1 0.6 add_compare_fusion.2
  400.8 0.7 fusion.115
  401.5 0.6 constant_dynamic-update-slice_fusion.2
  402.2 0.7 fusion.111
  402.9 5.4 %copy.134 = bf16[32,8,64,128]{3,2,1,0:T(8,128)(2,1)} copy(bf16[32,8,64,128]{3,1,2,0:T(8,128)(2,1)} %bitcast.247) | data formatting | bytes 8388608 | tf_op jit(solution)/shard_map/while
  408.3 2.8 gather_fusion
  412.5 0.7 fusion.113
  413.4 0.4 select_reduce_fusion.6
  414.2 0.6 dynamic_slice.78
  414.8 0.6 add_compare_fusion.2
  415.4 0.7 fusion.115
  416.2 0.6 constant_dynamic-update-slice_fusion.2
  416.9 11.3 %all_gather.7 = bf16[256,1024]{1,0:T(8,128)(2,1)S(1)} all-gather(bf16[256,256]{1,0:T(8,128)(2,1)} %bitcast.265), channel_id=1, replica_groups=mesh['kv_0'=32,'kv_1'=4,'kv_2'=2,'tp'=4] {'tp'}, dimensions={1}, use_global_device_ids=true | all-gather | bytes 655360 | tf_op jit(solution)/shard_map/all_gather | solution.py:199
  428.4 2.4 fusion.29
  (135 shorter events, 11.0 us)
Async XLA Ops:
  6.5 1.2 copy-start
  6.5 70.3 %copy-start.2 = (bf16[2048,128]{1,0:T(8,128)(2,1)S(1)}, bf16[2048,128]{1,0:T(8,128)(2,1)}, u32[]{:S(2)}) copy-start(bf16[2048,128]{1,0:T(8,128)(2,1)} %param.24) | copy-start | bytes 1572868
  6.5 341.1 %all-gather.3.cloned.1.call-start = ((), (), s32[]{:S(2)}) async-start(), calls=%async_computation | async-start | bytes 10526720 | tf_op jit(solution)/shard_map/all_gather | solution.py:29
  7.8 1.7 copy-start.4
  7.8 70.9 %copy-start.3 = (bf16[2048,128]{1,0:T(8,128)(2,1)S(1)}, bf16[2048,128]{1,0:T(8,128)(2,1)}, u32[]{:S(2)}) copy-start(bf16[2048,128]{1,0:T(8,128)(2,1)} %param.26) | copy-start | bytes 1572868
  9.4 71.9 %copy-start.1 = (bf16[2048,256]{1,0:T(8,128)(2,1)S(1)}, bf16[2048,256]{1,0:T(8,128)(2,1)}, u32[]{:S(2)}) copy-start(bf16[2048,256]{1,0:T(8,128)(2,1)} %param.18) | copy-start | bytes 3145732
  76.9 7.4 %copy-start.5 = (f32[64,32]{0,1:T(8,128)S(1)}, f32[64,32]{0,1:T(8,128)}, u32[]{:S(2)}) copy-start(f32[64,32]{0,1:T(8,128)} %copy-done.4) | copy-start | bytes 24580
  356.8 1.3 copy-start.7
  358.1 70.3 %copy-start.6 = (f32[1024]{0:T(1024)S(1)}, f32[1024]{0:T(1024)}, u32[]{:S(2)}) copy-start(f32[1024]{0:T(1024)} %param.28) | copy-start | bytes 12292
Sparse Core Ops, SparseCore 0:
  81.4 266.2 all-gather.2
where the time goes:
time: 440 us; the launch traced here: 438 us
  waiting for transfers between devices  263 us (60%)
  blocking collectives  68.9 us (16%)
  local copies, waits for them, and re-layouts  57.3 us (13%)
  matrix products  21.7 us (5%)
  between operations  13.7 us (3%)
  other arithmetic  12.3 us (3%)
    all_gather x1, waiting for transfers between devices, turned_gather(): filled = lax.all_gather(both, axis, axis=0, tiled=True)  263 us
    pmax x3, blocking collectives, by_axis(): return functools.reduce(lax.pmax, axes, array)  57.6 us
    while x4, local copies, waits for them, and re-layouts  21.4 us
    all_gather x1, blocking collectives, shards(): lax.all_gather(mixed, 'tp', axis=1, tiled=True).astype(jnp.float32)  11.3 us
    gather x8, local copies, waits for them, and re-layouts, one_sequence(): table[index]  11.2 us
    unnamed x19, local copies, waits for them, and re-layouts  9.29 us
  transfers between devices with their start and end apart: 1, of which 1 were waited for; matrix products, arithmetic and copies ran while one was open for 1% of the time, Pallas kernels for 0%

commit v1 on v0

v1 whole, which is shorter than its diff:
```python
import functools

import jax
import jax.numpy as jnp
from jax import lax
from jax.experimental import pallas as pl
from jax.experimental.pallas import tpu as pltpu
from jax.sharding import Mesh
from jax.sharding import PartitionSpec as P

HEADS = 16
HEAD_DIM = 64
CMP_STRIDE = 16
CMP_BLOCK = 32
TOPK = 16
KV = ("kv_0", "kv_1", "kv_2")
MESH = pl.DeviceIdType.MESH
ZS = 32
XS = 4
SPAN = 64
PIECE = 80
BLOCKS = 256

theta_base = 500000.0
norm_eps = 1e-06


def by_axis(array, axes):
    return functools.reduce(lax.pmax, axes, array)


def rotate(values, positions):
    width = values.shape[-1]
    half = width // 2
    inverse = jnp.exp(
        -jnp.log(jnp.float32(theta_base)) * jnp.arange(0, width, 2).astype(jnp.float32) / width
    )
    angle = positions.astype(jnp.float32)[:, None] * inverse[None, :]
    cosine = jnp.cos(angle)[:, None, :]
    sine = jnp.sin(angle)[:, None, :]
    first = values[..., :half]
    second = values[..., half:]
    return jnp.concatenate(
        [first * cosine - second * sine, second * cosine + first * sine], axis=-1
    )


def compress(raw, prior, weight_in, weight_out):
    seqs, span, groups, width = raw.shape
    extended = jnp.concatenate([prior, raw], axis=1)
    count = span // CMP_STRIDE
    front = extended[:, :span].reshape(seqs, count, CMP_STRIDE, groups, width)
    back = extended[:, CMP_STRIDE:].reshape(seqs, count, CMP_STRIDE, groups, width)
    window = jnp.concatenate([front, back], axis=2).transpose(0, 1, 3, 2, 4)
    window = window.reshape(seqs * count * groups, CMP_BLOCK * width)
    inner = jax.nn.gelu(jnp.dot(window, weight_in, preferred_element_type=jnp.float32)).astype(
        jnp.bfloat16
    )
    return jnp.dot(inner, weight_out, preferred_element_type=jnp.float32).reshape(
        seqs, count, groups, width
    )


def gather_kernel(piece, out, zsend, xsend, dsend, recv, local):
    z = lax.axis_index("kv_0")
    x = lax.axis_index("kv_1")
    c = lax.axis_index("kv_2")
    y = lax.axis_index("tp")
    right = lax.rem(x + 1, XS)
    left = lax.rem(x + XS - 1, XS)
    across = lax.rem(x + 2, XS)

    def zat(step):
        return lax.rem(z + step + ZS, ZS)

    def blk(zz, xx, cc):
        return (zz * XS + xx) * 2 + cc

    def copy(src, b, sem, device):
        return pltpu.make_async_remote_copy(
            src_ref=src,
            dst_ref=out.at[b],
            send_sem=sem,
            recv_sem=recv.at[b],
            device_id=device,
            device_id_type=MESH,
        )

    east = (z, right, c, y)
    west = (z, left, c, y)
    sibling = (z, x, 1 - c, y)

    barrier = pltpu.get_barrier_semaphore()
    partners = [(zat(s), x, c, y) for s in (1, -1, 2, -2)] + [east, west, sibling]
    for device in partners:
        pl.semaphore_signal(barrier, inc=1, device_id=device, device_id_type=MESH)
    pl.semaphore_wait(barrier, len(partners))

    me = blk(z, x, c)
    own = pltpu.make_async_copy(piece, out.at[me], local)
    own.start()
    for n, s in enumerate((1, -1, 2, -2)):
        copy(piece, me, zsend.at[n], (zat(s), x, c, y)).start()
    copy(piece, me, xsend.at[3 * z], east).start()
    copy(piece, me, xsend.at[3 * z + 1], west).start()
    copy(piece, me, dsend.at[z * XS + x], sibling).start()

    def arrive(b):
        copy(out.at[b], b, zsend.at[0], sibling).wait_recv()

    def across_core(zo, xo, b):
        copy(out.at[b], b, dsend.at[zo * XS + xo], sibling).start()

    def x_stage(zo, odd):
        b = blk(zo, left, c)
        arrive(b)
        if odd:
            copy(out.at[b], b, xsend.at[3 * zo + 2], east).start()
        across_core(zo, left, b)
        b = blk(zo, right, c)
        arrive(b)
        if not odd:
            copy(out.at[b], b, xsend.at[3 * zo + 2], west).start()
        across_core(zo, right, b)

    def o_stage(zo):
        b = blk(zo, across, c)
        arrive(b)
        across_core(zo, across, b)

    def each(r, use):
        use(2 * r - 1, 1, True)
        use(2 * r - 1, -1, True)
        use(2 * r, 1, False)

        @pl.when(r <= 7)
        def _():
            use(2 * r, -1, False)

    def body(r, carry):
        @pl.when(r <= 8)
        def _():
            def use(k, s, odd):
                zo = zat(-s * k)
                b = blk(zo, x, c)
                arrive(b)
                last = 7 if (s == 1 or odd) else 6

                @pl.when(r <= last)
                def _():
                    slot = 3 + k if s == 1 else 17 + k
                    copy(out.at[b], b, zsend.at[slot], (zat(2 * s), x, c, y)).start()

                copy(out.at[b], b, xsend.at[3 * zo], east).start()
                copy(out.at[b], b, xsend.at[3 * zo + 1], west).start()
                across_core(zo, x, b)

            each(r, use)

        @pl.when(r == 1)
        def _():
            x_stage(z, False)

        @pl.when((r >= 2) & (r <= 9))
        def _():
            each(r - 1, lambda k, s, odd: x_stage(zat(-s * k), odd))

        @pl.when(r == 2)
        def _():
            o_stage(z)

        @pl.when(r >= 3)
        def _():
            each(r - 2, lambda k, s, odd: o_stage(zat(-s * k)))

        return carry

    lax.fori_loop(1, 11, body, 0)

    def from_sibling(n, carry):
        arrive(n * 2 + 1 - c)
        return carry

    lax.fori_loop(0, ZS * XS, from_sibling, 0)
    own.wait()

    def sent(sem):
        def one(n, carry):
            copy(piece, me, sem.at[n], sibling).wait_send()
            return carry

        lax.fori_loop(0, sem.shape[0], one, 0)

    for sem in (zsend, xsend, dsend):
        sent(sem)


def gather_blocks(piece):
    sem = pltpu.SemaphoreType.DMA
    return pl.pallas_call(
        gather_kernel,
        out_shape=jax.ShapeDtypeStruct((BLOCKS, PIECE, 2 * HEAD_DIM), jnp.bfloat16),
        in_specs=[pl.BlockSpec(memory_space=pltpu.VMEM)],
        out_specs=pl.BlockSpec(memory_space=pltpu.VMEM),
        scratch_shapes=[
            sem((31,)),
            sem((3 * ZS,)),
            sem((XS * ZS,)),
            sem((BLOCKS,)),
            sem,
        ],
        compiler_params=pltpu.CompilerParams(collective_id=0, has_side_effects=True),
        name="gather_blocks",
    )(piece)


def softmax_weights(scores, valid):
    top = jnp.max(jnp.where(valid, scores, -1e30), axis=-1, keepdims=True)
    expd = jnp.where(valid, jnp.exp(scores - top), 0.0)
    total = jnp.sum(expd, axis=-1, keepdims=True)
    return (expd * (1.0 / jnp.maximum(total, 1.0))).astype(jnp.bfloat16)


NT = (((1,), (1,)), ((), ()))


def attention_kernel(place, lengths, picks, q_ref, own_ref, gate_ref, table, out, entries, pairs):
    s = pl.program_id(0)
    start = place[0] * SPAN
    count = SPAN // CMP_STRIDE
    width = 2 * HEAD_DIM

    @pl.when(s == 0)
    def _():
        def widen(n, carry):
            part = table[pl.ds(n * 16, 16), SPAN:PIECE, :]
            entries[pl.ds(n * 256, 256), :] = part.reshape(256, width).astype(jnp.float32)
            return carry

        lax.fori_loop(0, BLOCKS // 16, widen, 0)

    live = start < lengths[s]

    @pl.when(jnp.logical_not(live))
    def _():
        out[...] = jnp.zeros_like(out)

    @pl.when(live)
    def _():
        q = q_ref[0]
        rows = q.shape[0]
        cmp_pairs = jnp.concatenate(
            [
                entries[pl.ds(s * count + j, BLOCKS, stride=4 * count), :].astype(jnp.bfloat16)
                for j in range(count)
            ],
            axis=0,
        )
        total = BLOCKS * count
        scores = lax.dot_general(q, cmp_pairs, NT, preferred_element_type=jnp.float32)
        column = lax.broadcasted_iota(jnp.int32, (1, total), 1)
        entry = (column & (BLOCKS - 1)) * count + (column >> 8)
        entry_end = jnp.where(entry >= 1, entry * CMP_STRIDE + CMP_STRIDE - 1, 1 << 30)
        within = lax.broadcasted_iota(jnp.int32, (rows, 1), 0) & (SPAN - 1)
        weights = softmax_weights(scores, entry_end <= within + start)
        cmp_out = jnp.dot(weights, cmp_pairs, preferred_element_type=jnp.float32)

        pairs[0:SPAN, :] = own_ref[0]
        lane = lax.broadcasted_iota(jnp.int32, (1, TOPK * SPAN), 1)
        limit = jnp.where(lane < SPAN, lane, 0)
        for n in range(1, TOPK):
            pick = picks[s * TOPK + n]
            pairs[n * SPAN : (n + 1) * SPAN, :] = table[jnp.maximum(pick, 0), 0:SPAN, :]
            dead = jnp.where(pick < 0, 1 << 20, 0)
            limit = jnp.where((lane >> 6) == n, dead, limit)
        chosen_pairs = pairs[...]
        scores = lax.dot_general(q, chosen_pairs, NT, preferred_element_type=jnp.float32)
        weights = softmax_weights(scores, limit <= within)
        sel_out = jnp.dot(weights, chosen_pairs, preferred_element_type=jnp.float32)
        gate = gate_ref[0]
        mixed = gate[:, 0:1] * cmp_out + gate[:, 1:2] * sel_out
        mixed = jnp.where(within + start < lengths[s], mixed, 0.0).astype(jnp.bfloat16)
        mixed = mixed[:, HEAD_DIM:]
        out[0] = jnp.concatenate(
            [mixed[h * SPAN : (h + 1) * SPAN] for h in range(rows // SPAN)], axis=1
        )


def attention(place, lengths, picks, q, own, gates, table):
    seqs, rows, width = q.shape
    return pl.pallas_call(
        attention_kernel,
        out_shape=jax.ShapeDtypeStruct((seqs, SPAN, rows), jnp.bfloat16),
        grid_spec=pltpu.PrefetchScalarGridSpec(
            num_scalar_prefetch=3,
            grid=(seqs,),
            in_specs=[
                pl.BlockSpec((1, rows, width), lambda s, *_: (s, 0, 0)),
                pl.BlockSpec((1, SPAN, width), lambda s, *_: (s, 0, 0)),
                pl.BlockSpec((1, rows, 2), lambda s, *_: (s, 0, 0)),
                pl.BlockSpec(table.shape, lambda s, *_: (0, 0, 0)),
            ],
            out_specs=pl.BlockSpec((1, SPAN, rows), lambda s, *_: (s, 0, 0)),
            scratch_shapes=[
                pltpu.VMEM((BLOCKS * 16, width), jnp.float32),
                pltpu.VMEM((TOPK * SPAN, width), jnp.bfloat16),
            ],
        ),
        compiler_params=pltpu.CompilerParams(vmem_limit_bytes=48 << 20),
        name="attention",
    )(place, lengths, picks, q, own, gates, table)


def shards(
    hidden_in,
    w_query,
    w_cmp_key,
    w_cmp_value,
    w_sel_key,
    w_sel_value,
    w_gate,
    cmp_key_in,
    cmp_key_out,
    cmp_value_in,
    cmp_value_out,
    out_gain,
    w_out,
    seq_lengths,
    chosen,
):
    seqs, span, width = hidden_in.shape
    block_list = lax.axis_size(KV)
    place = lax.axis_index(KV)
    column = lax.axis_index("tp")
    local_heads = w_query.shape[1] // HEAD_DIM
    local_groups = w_sel_key.shape[1] // HEAD_DIM
    count = span // CMP_STRIDE
    scale = HEAD_DIM ** (-0.5)
    rows = hidden_in.reshape(seqs * span, width)
    positions = place * span + jnp.arange(span, dtype=jnp.int32)

    def project(weight_matrix, heads):
        return jnp.dot(rows, weight_matrix, preferred_element_type=jnp.float32).reshape(
            seqs, span, heads, HEAD_DIM
        )

    queries = rotate(project(w_query, local_heads), positions).astype(jnp.bfloat16)
    queries = jnp.transpose(queries, (0, 2, 1, 3)).reshape(seqs, local_heads * span, HEAD_DIM)
    queries = jnp.pad(queries * jnp.bfloat16(scale), ((0, 0), (0, 0), (0, HEAD_DIM)))
    sel_pairs = jnp.concatenate(
        [rotate(project(w_sel_key, local_groups), positions), project(w_sel_value, local_groups)],
        axis=-1,
    ).astype(jnp.bfloat16)
    raw_pairs = jnp.concatenate(
        [project(w_cmp_key, local_groups), project(w_cmp_value, local_groups)], axis=-1
    ).astype(jnp.bfloat16)
    prior = jnp.zeros((seqs, CMP_STRIDE, local_groups, HEAD_DIM), jnp.bfloat16)
    ends = place * span + jnp.arange(count, dtype=jnp.int32) * CMP_STRIDE + CMP_STRIDE - 1
    cmp_keys = rotate(compress(raw_pairs[..., :HEAD_DIM], prior, cmp_key_in, cmp_key_out), ends)
    cmp_values = compress(raw_pairs[..., HEAD_DIM:], prior, cmp_value_in, cmp_value_out)
    cmp_piece = jnp.concatenate(
        [cmp_keys.astype(jnp.bfloat16), cmp_values.astype(jnp.bfloat16)], axis=-1
    ).reshape(seqs * count, 2 * HEAD_DIM)
    picks = chosen[:, 0, 0]
    wanted = jnp.any(
        picks[:, 1:, None] == jnp.arange(block_list, dtype=jnp.int32), axis=1
    ).astype(jnp.int32)
    wanted = by_axis(wanted, KV)
    named = lax.dynamic_index_in_dim(wanted, place, axis=1, keepdims=False)
    seq_ids = jnp.arange(seqs, dtype=jnp.int32)
    exported_seq = jnp.sum(named * seq_ids)
    own = sel_pairs.reshape(seqs, span, 2 * HEAD_DIM)
    export = lax.dynamic_index_in_dim(own, exported_seq, axis=0, keepdims=False)
    table = gather_blocks(jnp.concatenate([export, cmp_piece], axis=0))
    gate_all = jnp.dot(rows, w_gate.reshape(width, 2 * HEADS), preferred_element_type=jnp.float32)
    gate_all = gate_all.reshape(seqs, span, 2, HEADS)
    gates = jax.nn.sigmoid(lax.dynamic_slice_in_dim(gate_all, column * local_heads, local_heads, 3))
    gates = jnp.transpose(gates, (0, 3, 1, 2)).reshape(seqs, local_heads * span, 2)
    mixed = attention(
        place.astype(jnp.int32).reshape(1), seq_lengths, picks.reshape(-1), queries, own, gates, table
    )
    mixed = mixed.reshape(seqs * span, local_heads * HEAD_DIM)
    out_width = width // lax.axis_size("tp")
    own_columns = lax.dynamic_slice_in_dim(w_out, column * out_width, out_width, 1)
    piece_wide = lax.all_gather(mixed, "tp", axis=1, tiled=True).astype(jnp.float32)
    scaled_piece = (piece_wide * out_gain[None, :]).astype(jnp.bfloat16)
    total = jnp.dot(scaled_piece, own_columns, preferred_element_type=jnp.float32)
    squares = jnp.sum(piece_wide * piece_wide, axis=-1)
    row_scale = lax.rsqrt(squares / (HEADS * HEAD_DIM) + norm_eps)
    return (total * row_scale[:, None]).astype(jnp.bfloat16).reshape(seqs, span, out_width)


def solution(mesh):
    torus = Mesh(mesh.devices.reshape(32, 4, 2, mesh.shape["tp"]), ("kv_0", "kv_1", "kv_2", "tp"))
    return jax.shard_map(
        shards,
        mesh=torus,
        in_specs=(
            P(None, KV, None),
            P(None, "tp"),
            P(None, "tp"),
            P(None, "tp"),
            P(None, "tp"),
            P(None, "tp"),
            P(),
            P(),
            P(),
            P(),
            P(),
            P(),
            P(),
            P(),
            P(None, KV, "tp", None),
        ),
        out_specs=P(None, KV, "tp"),
        check_vma=False,
    )
```

time: 440 us -> 159 us (0.36)
  waiting for transfers between devices: 263 us -> 0 us
  Pallas kernels: 0 us -> 60.9 us
  local copies, waits for them, and re-layouts: 57.3 us -> 6.55 us
  between operations: 13.7 us -> 2.26 us
  matrix products: 21.7 us -> 13.8 us
  other arithmetic: 12.3 us -> 5.54 us
    all_gather x1 -> x0, waiting for transfers between devices: 263 us -> none  [turned_gather(): filled = lax.all_gather(both, axis, axis=0, tiled=True)]
    pallas_call x0 -> x2, Pallas kernels: none -> 60.9 us  [the longest x1 50.9 us: gather_blocks(): pl.pallas_call(gather_kernel, out_shape=jax.ShapeDtypeStruct((BLOCKS, PIE...]
    while x4 -> x0, local copies, waits for them, and re-layouts: 21.4 us -> none
    gather x8 -> x0, local copies, waits for them, and re-layouts: 11.2 us -> none  [one_sequence(): table[index]]
    dot_general x16 -> x0, matrix products: 8.94 us -> none  [the longest x4 2.76 us: one_sequence(): jnp.einsum('ghqe,egd->qghd', weights, entries[..., HEAD_DIM:], preferred_...]
    unnamed x19 -> x22, local copies, waits for them, and re-layouts: 9.29 us -> 2 us
  transfers between devices with their start and end apart: 1 -> 0, of which waited for: 1 -> 0; matrix products, arithmetic and copies ran while one was open for 1% -> 0% of each run, Pallas kernels for 0% -> 0%
where the time goes in v1:
time: 159 us; the launch traced here: 158 us
  blocking collectives  68.6 us (43%)
  Pallas kernels  60.9 us (38%)
  matrix products  13.8 us (9%)
  local copies, waits for them, and re-layouts  6.55 us (4%)
  other arithmetic  5.54 us (3%)
  between operations  2.26 us (1%)
    pmax x3, blocking collectives, by_axis(): return functools.reduce(lax.pmax, axes, array)  57.6 us
    pallas_call x1, Pallas kernels, gather_blocks(): pl.pallas_call(gather_kernel, out_shape=jax.ShapeDtypeStruct((BLOCKS, PIE...  50.9 us
    all_gather x1, blocking collectives, shards(): lax.all_gather(mixed, 'tp', axis=1, tiled=True).astype(jnp.float32)  10.9 us
    pallas_call x1, Pallas kernels, attention(): pl.pallas_call(attention_kernel, out_shape=jax.ShapeDtypeStruct((seqs, SP...  9.98 us
    dot_general x5, matrix products, project(): jnp.dot(rows, weight_matrix, preferred_element_type=jnp.float32)  7.92 us

profile of v1, /device:TPU:1, one launch (start us, length us, event | category | flops | bytes accessed | tf_op | source)
XLA Modules:
  0.0 157.6 jit_solution(1105237643165759639)
XLA Ops:
  0.0 0.0 copy-start
  0.1 0.5 broadcast.175
  0.6 1.4 reduce.5
  2.0 0.1 reshape_squeeze.3.picks
  2.1 0.8 slice.33
  2.8 0.1 multiply_cosine_fusion.1
  2.9 0.1 copy.60
  3.0 0.1 fusion.16
  3.1 42.0 %pmax.21 = s32[4,256]{1,0:T(4,128)S(1)} all-reduce(s32[4,256]{1,0:T(4,128)S(1)} %convert_element_type.78), channel_id=1, replica_groups=mesh['kv_0'=32,'kv_1'=4,'kv_2'=2,'tp'=4] {'kv_0'}, use_global_device_ids=true, to_apply=%region_1.2 | all-reduce | flops 1024 | bytes 8192 | tf_op jit(solution)/shard_map/pmax | solution.py:29
  45.1 7.2 %pmax.22 = s32[4,256]{1,0:T(4,128)S(1)} all-reduce(s32[4,256]{1,0:T(4,128)S(1)} %pmax.21), channel_id=1, replica_groups=mesh['kv_0'=32,'kv_1'=4,'kv_2'=2,'tp'=4] {'kv_1'}, use_global_device_ids=true, to_apply=%region_2.3 | all-reduce | flops 1024 | bytes 8192 | tf_op jit(solution)/shard_map/pmax | solution.py:29
  52.3 8.5 %pmax.23 = s32[4,256]{1,0:T(4,128)S(1)} all-reduce(s32[4,256]{1,0:T(4,128)S(1)} %pmax.22), channel_id=1, replica_groups=mesh['kv_0'=32,'kv_1'=4,'kv_2'=2,'tp'=4] {'kv_2'}, use_global_device_ids=true, to_apply=%region_3.4 | all-reduce | flops 1024 | bytes 8192 | tf_op jit(solution)/shard_map/pmax | solution.py:29
  60.8 0.2 dynamic-slice_reduce_fusion
  60.9 0.6 multiply_reduce_fusion
  63.5 0.1 multiply_cosine_fusion
  63.7 0.0 copy-start.5
  63.7 0.0 copy-start.7
  63.7 0.7 copy.57
  64.4 0.7 copy.58
  65.1 0.0 copy-done
  65.1 1.6 convolution_convert_fusion.1
  66.6 1.6 convolution_convert_fusion
  68.2 0.0 copy-done.5
  68.2 0.0 copy-done.7
  68.2 0.0 copy-start.2
  68.2 1.5 convolution_convert_fusion.2
  69.7 0.1 pad_slice_fusion
  69.8 0.1 copy.63
  69.9 0.7 copy.64
  70.6 0.9 pad_maximum_fusion.1
  71.5 0.2 reshape_transpose.7
  71.7 0.0 copy-done.3
  71.7 1.0 convolution_convert_fusion.3
  72.7 0.1 pad_slice_fusion.1
  72.8 0.1 copy.61
  72.9 0.1 copy.62
  73.1 0.2 reshape_transpose.6
  73.3 0.0 copy-done.4
  73.3 1.0 fusion.37
  74.3 0.1 subtract_convert_fusion.2
  74.4 1.5 fusion.3
  75.9 0.0 copy-start.6
  75.9 0.0 copy-start.8
  75.9 1.4 convolution_bitcast_fusion
  77.3 0.9 subtract_convert_fusion.1
  78.2 0.1 fusion.19
  78.3 0.7 maximum_maximum_fusion.piece
  79.0 0.1 pad_maximum_fusion.2.own_ref
  79.1 0.2 copy.59
  79.4 0.0 copy-done.2
  79.4 1.4 copy.54
  80.8 1.9 %fusion.5 = f32[4,64,4,64]{1,3,2,0:T(8,128)S(1)} fusion(bf16[4,64,2048,1]{2,1,0,3:T(8,128)(2,1)} %bitcast.81, bf16[4,64,2048]{2,1,0:T(8,128)(2,1)S(1)} %copy-done), kind=kOutput, calls=%fused_computation.13 | convolution fusion | flops 268435456 | bytes 2359296 | tf_op jit(solution)/shard_map/dot_general | solution.py:343
  82.8 0.0 copy-done.6
  82.8 0.0 copy-done.8
  82.8 0.0 copy-start.1
  82.8 0.1 subtract_convert_fusion
  82.9 0.1 fusion.10
  83.0 0.2 copy.55
  83.1 0.1 pad.6.q_ref
  83.2 50.9 %gather_blocks.1.table = bf16[256,80,128]{2,1,0:T(8,128)(2,1)} custom-call(bf16[80,128]{1,0:T(8,128)(2,1)} %maximum_maximum_fusion.piece), custom_call_target="tpu_custom_call" | custom-call | tf_op jit(solution)/shard_map/gather_blocks/pallas_call | solution.py:200
  134.1 0.0 copy-start.9
  134.1 10.0 %attention.1 = bf16[4,64,256]{2,1,0:T(8,128)(2,1)S(1)} custom-call(s32[1]{0:T(128)} %bitcast.place, s32[4]{0:T(128)S(1)} %copy-done.1, s32[64]{0:T(128)S(1)} %reshape_squeeze.3.picks, bf16[4,256,128]{2,1,0:T(8,128)(2,1)S(1)} %pad.6.q_ref, bf16[4,64,128]{2,1,0:T(8,128)(2,1)S(1)} %pad_maximum_fusion.2.own_ref, f32[4,256,2]{2,1,0:T(8,128)S(1)} %bitcast.78, ...), custom_call_target="tpu_custom_call" | custom-call | tf_op jit(solution)/shard_map/attention/pallas_call | solution.py:291
  144.1 10.9 %all_gather.3 = bf16[256,1024]{1,0:T(8,128)(2,1)S(1)} all-gather(bf16[256,256]{1,0:T(8,128)(2,1)S(1)} %bitcast.79), channel_id=1, replica_groups=mesh['kv_0'=32,'kv_1'=4,'kv_2'=2,'tp'=4] {'tp'}, dimensions={1}, use_global_device_ids=true | all-gather | bytes 655360 | tf_op jit(solution)/shard_map/all_gather | solution.py:385
  155.0 0.2 fusion.2
  155.2 2.4 %fusion = bf16[256,512]{1,0:T(8,128)(2,1)} fusion(bf16[1024,2048]{1,0:T(8,128)(2,1)} %param.27, s32[]{:T(128)S(6)} %select_n.17, bf16[256,1024]{1,0:T(8,128)(2,1)S(1)} %all_gather.3, f32[1024]{0:T(1024)S(1)} %copy-done.9, f32[256]{0:T(256)S(1)} %add_rsqrt_fusion), kind=kOutput, calls=%fused_computation.3 | convolution fusion | flops 269484032 | bytes 1840132 | tf_op jit(solution)/shard_map/dot_general | solution.py:387
  (11 shorter events, 0.1 us)
Async XLA Ops:
  0.0 65.1 %copy-start = (bf16[4,64,2048]{2,1,0:T(8,128)(2,1)S(1)}, bf16[4,64,2048]{2,1,0:T(8,128)(2,1)}, u32[]{:S(2)}) copy-start(bf16[4,64,2048]{2,1,0:T(8,128)(2,1)} %param.15) | copy-start | bytes 3145732
  0.0 71.7 %copy-start.3 = (bf16[2048,128]{1,0:T(8,128)(2,1)S(1)}, bf16[2048,128]{1,0:T(8,128)(2,1)}, u32[]{:S(2)}) copy-start(bf16[2048,128]{1,0:T(8,128)(2,1)} %param.24) | copy-start | bytes 1572868
  0.0 73.3 %copy-start.4 = (bf16[2048,128]{1,0:T(8,128)(2,1)S(1)}, bf16[2048,128]{1,0:T(8,128)(2,1)}, u32[]{:S(2)}) copy-start(bf16[2048,128]{1,0:T(8,128)(2,1)} %param.22) | copy-start | bytes 1572868
  63.7 4.5 %copy-start.5 = (f32[64,32]{0,1:T(8,128)}, f32[64,32]{0,1:T(8,128)S(1)}, u32[]{:S(2)}) copy-start(f32[64,32]{0,1:T(8,128)S(1)} %get-tuple-element.13) | copy-start | bytes 24580
  63.7 4.5 %copy-start.7 = (f32[64,32]{0,1:T(8,128)}, f32[64,32]{0,1:T(8,128)S(1)}, u32[]{:S(2)}) copy-start(f32[64,32]{0,1:T(8,128)S(1)} %get-tuple-element.14) | copy-start | bytes 24580
  68.2 11.1 %copy-start.2 = (bf16[2048,256]{1,0:T(8,128)(2,1)S(1)}, bf16[2048,256]{1,0:T(8,128)(2,1)}, u32[]{:S(2)}) copy-start(bf16[2048,256]{1,0:T(8,128)(2,1)} %param.16) | copy-start | bytes 3145732
  75.9 6.8 %copy-start.6 = (f32[64,32]{0,1:T(8,128)S(1)}, f32[64,32]{0,1:T(8,128)}, u32[]{:S(2)}) copy-start(f32[64,32]{0,1:T(8,128)} %copy-done.5) | copy-start | bytes 24580
  75.9 6.8 %copy-start.8 = (f32[64,32]{0,1:T(8,128)S(1)}, f32[64,32]{0,1:T(8,128)}, u32[]{:S(2)}) copy-start(f32[64,32]{0,1:T(8,128)} %copy-done.7) | copy-start | bytes 24580
  82.8 51.3 %copy-start.1 = (s32[4]{0:T(128)S(1)}, s32[4]{0:T(128)}, u32[]{:S(2)}) copy-start(s32[4]{0:T(128)} %lengths.1) | copy-start | bytes 52
  134.1 21.1 %copy-start.9 = (f32[1024]{0:T(1024)S(1)}, f32[1024]{0:T(1024)}, u32[]{:S(2)}) copy-start(f32[1024]{0:T(1024)} %param.26) | copy-start | bytes 12292
